TPU v7x, 32 devices: a whole 2x2x4 slice. The times are simulated.
32 devices in a mesh: sp: 8 (over z, x), tp: 4 (over y, core).
Axes of the slice: x: 2, y: 2, z: 4, core: 2. Of those that a mesh axis runs over, the one named last changes fastest.
Arguments:
- residual: bfloat16 [2048, 2048], P(('sp', 'tp')), may hold values from -6 to 6
- queries: bfloat16 [2048, 1024], P('sp', 'tp'), may hold values from -8 to 8
- key_pairs: bfloat16 [2048, 512], P('sp', 'tp'), may hold values from -8 to 8
- values: bfloat16 [2048, 512], P('sp', 'tp'), may hold values from -6 to 6
- lambdas: float32 [8], P('tp'), may hold values from 0.3 to 0.8
- head_gain: float32 [128], replicated, may hold values from 0.1 to 1.9
- out_weight: bfloat16 [1024, 2048], replicated, may hold values from -0.1875 to 0.1875
- mixer_gain: float32 [2048], replicated, may hold values from 0.1 to 1.9
- before_gain: float32 [2048], replicated, may hold values from 0.1 to 1.9
- after_gain: float32 [2048], replicated, may hold values from 0.1 to 1.9
- gate_weight: bfloat16 [2048, 5632], P('sp', 'tp'), may hold values from -0.125 to 0.125
- up_weight: bfloat16 [2048, 5632], P('sp', 'tp'), may hold values from -0.125 to 0.125
- down_weight: bfloat16 [5632, 2048], P('tp', 'sp'), may hold values from -0.078125 to 0.078125
Outputs:
- updated: bfloat16 [2048, 2048], P(('sp', 'tp'))
All inputs are finite; a program needn't handle non-finite values.
Results may differ from a plain program's by a relative error of at most 0.014.
Values may be sent and summed in bfloat16 or wider, within the bound.
A program may use at most 128 MiB of HBM per device.

v0:
```python
import math
import jax
import jax.numpy as jnp
from jax import lax
from jax.sharding import PartitionSpec as P

HEAD_DIM = 64


def row_norm(values_in, gain, epsilon):
    mean_square = jnp.mean(values_in * values_in, axis=-1, keepdims=True)
    return values_in * lax.rsqrt(mean_square + epsilon) * gain


def on_device(
    residual,
    queries,
    key_pairs,
    values,
    lambdas,
    head_gain,
    out_weight,
    mixer_gain,
    before_gain,
    after_gain,
    gate_weight,
    up_weight,
    down_weight,
):
    tokens_here = queries.shape[0]
    quarter = residual.shape[0]
    width = 2 * HEAD_DIM
    local_heads = queries.shape[1] // width
    scale = 1.0 / math.sqrt(HEAD_DIM)
    height = local_heads * tokens_here
    query_rows = jnp.transpose(
        queries.reshape(tokens_here, local_heads, 2, HEAD_DIM), (2, 1, 0, 3)
    ).reshape(2, height, HEAD_DIM)
    empty = (
        jnp.full((height,), -1e30, jnp.float32),
        jnp.zeros((height,), jnp.float32),
        jnp.zeros((height, width), jnp.float32),
    )
    state = (empty, empty)
    key_piece = lax.all_gather(key_pairs, "sp", axis=0, tiled=True)
    value_piece = lax.all_gather(values, "sp", axis=0, tiled=True)
    length = key_piece.shape[0]
    span = length
    for split_count in range(1, length + 1):
        if length % split_count == 0 and length // split_count <= 2048:
            span = length // split_count
            break
    key_blocks = key_piece.reshape(length // span, span, 2, HEAD_DIM)
    value_blocks = value_piece.reshape(length // span, span, width)

    def advance(carry, blocks_in):
        key_block, value_block = blocks_in
        renewed = []
        for which in range(2):
            running_top, running_total, running_numer = carry[which]
            score = (
                jnp.dot(
                    query_rows[which], key_block[:, which].T, preferred_element_type=jnp.float32
                )
                * scale
            )
            new_top = jnp.maximum(running_top, jnp.max(score, axis=1))
            shrink = jnp.exp(running_top - new_top)
            expo = jnp.exp(score - new_top[:, None])
            new_total = running_total * shrink + jnp.sum(expo, axis=1)
            new_numer = running_numer * shrink[:, None] + jnp.dot(
                expo.astype(jnp.bfloat16), value_block, preferred_element_type=jnp.float32
            )
            renewed.append((new_top, new_total, new_numer))
        return (tuple(renewed), None)

    state, _ = lax.scan(advance, state, (key_blocks, value_blocks))
    first_map, second_map = state
    lambda_rows = jnp.repeat(lambdas, tokens_here)[:, None]
    attended = first_map[2] / first_map[1][:, None] - lambda_rows * (
        second_map[2] / second_map[1][:, None]
    )
    normed = row_norm(attended, head_gain, 1e-05).astype(jnp.bfloat16)
    head_out = jnp.transpose(normed.reshape(local_heads, tokens_here, width), (1, 0, 2)).reshape(
        tokens_here, local_heads * width
    )
    grouped = head_out.reshape(lax.axis_size("tp"), quarter, local_heads * width)
    mixed = jnp.dot(
        lax.all_to_all(grouped, "tp", split_axis=0, concat_axis=2, tiled=True)[0],
        out_weight,
        preferred_element_type=jnp.float32,
    ).astype(jnp.bfloat16)[None][0]
    stream = residual.astype(jnp.float32) + row_norm(mixed.astype(jnp.float32), mixer_gain, 1e-06)
    normed_in = row_norm(stream, before_gain, 1e-06).astype(jnp.bfloat16)
    gathered = lax.all_gather(normed_in, "tp", axis=0, tiled=True)
    empty_hidden = jnp.zeros((gathered.shape[0], gate_weight.shape[1]), jnp.float32)
    pieces = (
        lax.all_gather(gate_weight, "sp", axis=0, tiled=True),
        lax.all_gather(up_weight, "sp", axis=0, tiled=True),
    )
    columns = lax.slice_in_dim(gathered, 0, pieces[0].shape[0], axis=1)
    gate_part = jnp.dot(columns, pieces[0], preferred_element_type=jnp.float32)
    up_part = jnp.dot(columns, pieces[1], preferred_element_type=jnp.float32)
    gate = empty_hidden + gate_part
    up = empty_hidden + up_part
    down_whole = lax.all_gather(down_weight, "sp", axis=1, tiled=True)
    hidden = (jax.nn.silu(gate) * up).astype(jnp.bfloat16)
    picked = lax.slice_in_dim(hidden, 0, lax.axis_size("tp") * quarter, axis=0)
    channel = lax.psum_scatter(
        jnp.dot(picked, down_whole, preferred_element_type=jnp.float32).astype(jnp.bfloat16),
        "tp",
        scatter_dimension=0,
        tiled=True,
    )
    updated = stream + 0.5 * row_norm(channel.astype(jnp.float32), after_gain, 1e-06)
    return updated.astype(jnp.bfloat16)


def solution(mesh):
    return jax.shard_map(
        on_device,
        mesh=mesh,
        in_specs=(
            P(("sp", "tp"), None),
            P("sp", "tp"),
            P("sp", "tp"),
            P("sp", "tp"),
            P("tp"),
            P(),
            P(),
            P(),
            P(),
            P(),
            P("sp", "tp"),
            P("sp", "tp"),
            P("tp", "sp"),
        ),
        out_specs=P(("sp", "tp"), None),
        check_vma=False,
    )
```

profile of v0, /device:TPU:0, one launch (start us, length us, event | category | flops | bytes accessed | tf_op | source)
XLA Modules:
  0.0 430.2 jit_solution(3633528644462433819)
XLA Ops:
  6.5 0.0 copy-start
  6.5 0.9 copy.16
  7.5 33.0 %all_gather.18 = bf16[2048,128]{0,1:T(8,128)(2,1)S(1)} all-gather(bf16[256,128]{0,1:T(8,128)(2,1)S(1)} %copy.16), channel_id=1, replica_groups=mesh['sp'=8,'tp'=4] {'sp'}, dimensions={0}, use_global_device_ids=true | all-gather | bytes 589824 | tf_op jit(solution)/shard_map/all_gather | solution.py:45
  40.5 1.0 copy.14
  41.6 0.1 copy.15
  41.7 0.0 copy-start.3
  41.7 0.8 multiply_reduce_fusion.1
  42.5 0.8 fusion
  43.3 31.3 %all_gather.19 = bf16[2048,128]{1,0:T(8,128)(2,1)S(1)} all-gather(bf16[256,128]{1,0:T(8,128)(2,1)S(1)} %copy-done.3), channel_id=1, replica_groups=mesh['sp'=8,'tp'=4] {'sp'}, dimensions={0}, use_global_device_ids=true | all-gather | bytes 589824 | tf_op jit(solution)/shard_map/all_gather | solution.py:46
  74.6 0.1 copy.17
  74.7 0.8 multiply_reduce_fusion
  75.5 0.8 fusion.2
  76.4 0.0 copy-done
  76.4 0.1 broadcast_bitcast_fusion
  76.5 0.9 fusion.29
  77.3 0.0 copy-start.6
  77.4 1.5 multiply_reduce_fusion.4
  78.8 0.0 copy-start.1
  78.9 0.0 copy-start.2
  78.9 0.0 copy-start.4
  78.9 0.1 multiply_convert_fusion.1
  79.0 0.1 copy.25
  79.2 0.1 reshape_reshape.3
  79.3 7.2 %all_to_all.15 = bf16[4,64,256]{2,1,0:T(8,128)(2,1)S(1)} all-to-all(bf16[4,64,256]{2,1,0:T(8,128)(2,1)S(1)} %reshape_reshape.3), channel_id=1, replica_groups=mesh['sp'=8,'tp'=4] {'tp'}, dimensions={0} | all-to-all | bytes 262144 | tf_op jit(solution)/shard_map/all_to_all | solution.py:89
  86.5 0.1 copy.19
  86.6 3.1 multiply_reduce_fusion.3
  89.8 0.0 copy-done.2
  89.8 0.3 multiply_reduce_fusion.2
  90.1 0.9 multiply_convert_fusion
  91.0 0.0 all-gather.5.cloned.1.call-update
  91.0 0.0 all-gather.7.cloned.1.call-start
  91.0 0.7 all-gather.7.cloned.1.call-update
  91.8 0.0 all-gather.11.cloned.1.call-start
  91.8 0.7 all-gather.11.cloned.1.call-update
  92.5 0.0 all-gather.9.cloned.1.call-start
  92.5 0.5 all-gather.9.cloned.1.call-update
  93.1 0.0 reduce-scatter.2.cloned.1.call-start
  93.1 15.0 %all-gather.5.cloned.1.call-done = bf16[256,2048]{1,0:T(8,128)(2,1)} async-done(((bf16[64,2048]{1,0:T(8,128)(2,1)}), bf16[256,2048]{1,0:T(8,128)(2,1)}) %all-gather.5.cloned.1.call-update) | async-done | bytes 1048592 | tf_op jit(solution)/shard_map/all_gather | solution.py:95
  108.1 94.5 %all-gather.7.cloned.1.call-done = bf16[2048,1408]{1,0:T(8,128)(2,1)} async-done(((bf16[256,1408]{1,0:T(8,128)(2,1)}), bf16[2048,1408]{1,0:T(8,128)(2,1)}) %all-gather.7.cloned.1.call-update) | async-done | bytes 5767184 | tf_op jit(solution)/shard_map/all_gather | solution.py:98
  202.6 4.8 %fusion.45 = f32[256,1408]{1,0:T(8,128)S(1)} fusion(bf16[256,2048]{1,0:T(8,128)(2,1)} %all-gather.5.cloned.1.call-done, bf16[2048,1408]{1,0:T(8,128)(2,1)} %all-gather.7.cloned.1.call-done), kind=kOutput, calls=%fused_computation.58 | convolution fusion | flops 1476395008 | bytes 8257536 | tf_op jit(solution)/shard_map/dot_general | solution.py:102
  207.4 0.0 copy-start.5
  207.4 88.6 %all-gather.11.cloned.1.call-done = bf16[1408,2048]{1,0:T(8,128)(2,1)} async-done(((bf16[1408,256]{1,0:T(8,128)(2,1)}), bf16[1408,2048]{1,0:T(8,128)(2,1)}) %all-gather.11.cloned.1.call-update) | async-done | bytes 5767184 | tf_op jit(solution)/shard_map/all_gather | solution.py:106
  296.0 92.6 %all-gather.9.cloned.1.call-done = bf16[2048,1408]{1,0:T(8,128)(2,1)} async-done(((bf16[256,1408]{1,0:T(8,128)(2,1)}), bf16[2048,1408]{1,0:T(8,128)(2,1)}) %all-gather.9.cloned.1.call-update) | async-done | bytes 5767184 | tf_op jit(solution)/shard_map/all_gather | solution.py:99
  388.6 8.9 %convolution_convert_fusion = bf16[256,2048]{1,0:T(8,128)(2,1)} fusion(bf16[1408,2048]{1,0:T(8,128)(2,1)} %all-gather.11.cloned.1.call-done, bf16[256,2048]{1,0:T(8,128)(2,1)S(1)} %copy-done.7, bf16[2048,1408]{1,0:T(8,128)(2,1)} %all-gather.9.cloned.1.call-done, f32[256,1408]{1,0:T(8,128)S(1)} %fusion.45), kind=kOutput, calls=%fused_computation.10 | convolution fusion | flops 2955476992 | bytes 15073280 | tf_op jit(solution)/shard_map/dot_general | solution.py:110
  397.5 0.0 reduce-scatter.2.cloned.1.call-update
  397.5 23.1 %reduce-scatter.2.cloned.1.call-done = bf16[64,2048]{1,0:T(8,128)(2,1)} async-done(((bf16[256,2048]{1,0:T(8,128)(2,1)}), bf16[64,2048]{1,0:T(8,128)(2,1)}) %reduce-scatter.2.cloned.1.call-update) | async-done | bytes 262160 | tf_op jit(solution)/shard_map/reduce_scatter | solution.py:109
  420.6 1.1 fusion.32
  421.7 1.9 fusion.36
  (21 shorter events, 0.1 us)
Async XLA Ops:
  6.5 69.8 %copy-start = (f32[2]{0:T(128)S(1)}, f32[2]{0:T(128)}, u32[]{:S(2)}) copy-start(f32[2]{0:T(128)} %param.17) | copy-start | bytes 28
  6.5 101.6 %all-gather.5.cloned.1.call-start = ((), (), s32[]{:S(2)}) async-start(), calls=%async_computation.2 | async-start | bytes 1310720 | tf_op jit(solution)/shard_map/all_gather | solution.py:95
  41.7 1.7 copy-start.3
  77.3 1.6 copy-start.6
  78.8 10.9 %copy-start.1 = (bf16[64,2048]{1,0:T(8,128)(2,1)S(1)}, bf16[64,2048]{1,0:T(8,128)(2,1)}, u32[]{:S(2)}) copy-start(bf16[64,2048]{1,0:T(8,128)(2,1)} %param.13) | copy-start | bytes 786436
  78.9 10.9 %copy-start.2 = (f32[2048]{0:T(1024)S(1)}, f32[2048]{0:T(1024)}, u32[]{:S(2)}) copy-start(f32[2048]{0:T(1024)} %param.20) | copy-start | bytes 24580
  78.9 11.2 %copy-start.4 = (f32[2048]{0:T(1024)S(1)}, f32[2048]{0:T(1024)}, u32[]{:S(2)}) copy-start(f32[2048]{0:T(1024)} %param.21) | copy-start | bytes 24580
  91.0 111.6 %all-gather.7.cloned.1.call-start = ((), (), s32[]{:S(2)}) async-start(), calls=%async_computation.3 | async-start | bytes 6488064 | tf_op jit(solution)/shard_map/all_gather | solution.py:98
  91.8 204.3 %all-gather.11.cloned.1.call-start = ((), (), s32[]{:S(2)}) async-start(), calls=%async_computation.5 | async-start | bytes 6488064 | tf_op jit(solution)/shard_map/all_gather | solution.py:106
  92.5 296.1 %all-gather.9.cloned.1.call-start = ((), (), s32[]{:S(2)}) async-start(), calls=%async_computation.4 | async-start | bytes 6488064 | tf_op jit(solution)/shard_map/all_gather | solution.py:99
  93.1 327.5 %reduce-scatter.2.cloned.1.call-start = ((), (), s32[]{:S(2)}) async-start(), calls=%async_computation.6 | async-start | bytes 1310720 | tf_op jit(solution)/shard_map/reduce_scatter | solution.py:109
  108.1 280.5 %copy-start.7 = (bf16[256,2048]{1,0:T(8,128)(2,1)S(1)}, bf16[256,2048]{1,0:T(8,128)(2,1)}, u32[]{:S(2)}) copy-start(bf16[256,2048]{1,0:T(8,128)(2,1)} %all-gather.5.cloned.1.call-done) | copy-start | bytes 3145732
  207.4 214.3 %copy-start.5 = (f32[2048]{0:T(1024)S(1)}, f32[2048]{0:T(1024)}, u32[]{:S(2)}) copy-start(f32[2048]{0:T(1024)} %param.22) | copy-start | bytes 24580
Sparse Core Ops, SparseCore 0:
  91.1 16.9 all-gather.4
  110.3 92.2 all-gather.6
  204.7 91.2 all-gather.10
  298.1 90.4 all-gather.8
  397.6 22.9 reduce-scatter.1
where the time goes:
time: 431 us; the launch traced here: 430 us
  waiting for transfers between devices  316 us (73%)
  blocking collectives  71.5 us (17%)
  matrix products  20.8 us (5%)
  between operations  13.4 us (3%)
  other arithmetic  6.02 us (1%)
    all_gather x1, waiting for transfers between devices, on_device(): lax.all_gather(gate_weight, 'sp', axis=0, tiled=True)  94.5 us
    all_gather x1, waiting for transfers between devices, on_device(): lax.all_gather(up_weight, 'sp', axis=0, tiled=True)  92.6 us
    all_gather x1, waiting for transfers between devices, on_device(): down_whole = lax.all_gather(down_weight, 'sp', axis=1, tiled=True)  88.6 us
    all_gather x1, blocking collectives, on_device(): key_piece = lax.all_gather(key_pairs, 'sp', axis=0, tiled=True)  33 us
    all_gather x1, blocking collectives, on_device(): value_piece = lax.all_gather(values, 'sp', axis=0, tiled=True)  31.3 us
    reduce_scatter x1, waiting for transfers between devices, on_device(): lax.psum_scatter(jnp.dot(picked, down_whole, preferred_element_type=jnp.f...  23.1 us
    all_gather x1, waiting for transfers between devices, on_device(): gathered = lax.all_gather(normed_in, 'tp', axis=0, tiled=True)  15 us
    dot_general x1, matrix products, on_device(): jnp.dot(picked, down_whole, preferred_element_type=jnp.float32)  8.9 us
  transfers between devices with their start and end apart: 5, of which 5 were waited for; matrix products, arithmetic and copies ran while one was open for 1% of the time, Pallas kernels for 0%

commit v1 on v0

--- a/solution.py
+++ b/solution.py
@@ -5,6 +5,13 @@
 from jax.sharding import PartitionSpec as P
 
 HEAD_DIM = 64
+
+
+def end_stops_all(view, content):
+    new = jnp.concatenate([view, content], axis=1)
+    out_arr = lax.all_gather(new, axis_name="sp", axis=0, tiled=True)
+    w1 = jnp.split(out_arr, [view.shape[1]], axis=1)
+    return w1
 
 
 def row_norm(values_in, gain, epsilon):
@@ -42,8 +49,7 @@
         jnp.zeros((height, width), jnp.float32),
     )
     state = (empty, empty)
-    key_piece = lax.all_gather(key_pairs, "sp", axis=0, tiled=True)
-    value_piece = lax.all_gather(values, "sp", axis=0, tiled=True)
+    key_piece, value_piece = end_stops_all(key_pairs, values)
     length = key_piece.shape[0]
     span = length
     for split_count in range(1, length + 1):

time: 431 us -> 407 us (0.944)
  blocking collectives: 71.5 us -> 7.26 us
  waiting for transfers between devices: 316 us -> 354 us
    all_gather x2 -> x0, blocking collectives: 64.3 us -> none  [the longest x1 33 us: on_device(): key_piece = lax.all_gather(key_pairs, 'sp', axis=0, tiled=True)]
    all_gather x0 -> x1, waiting for transfers between devices: none -> 41 us  [end_stops_all(): out_arr = lax.all_gather(new, axis_name='sp', axis=0, tiled=True)]
    all_gather x1, waiting for transfers between devices: 92.6 us -> 87.8 us  [on_device(): lax.all_gather(up_weight, 'sp', axis=0, tiled=True)]
    all_gather x1, waiting for transfers between devices: 88.6 us -> 93.2 us  [on_device(): down_whole = lax.all_gather(down_weight, 'sp', axis=1, tiled=True)]
  transfers between devices with their start and end apart: 5 -> 6, of which waited for: 5 -> 6; matrix products, arithmetic and copies ran while one was open for 1% -> 1% of each run, Pallas kernels for 0% -> 0%
where the time goes in v1:
time: 407 us
  waiting for transfers between devices  354 us (87%)
  matrix products  20.4 us (5%)
  between operations  13.7 us (3%)
  blocking collectives  7.26 us (2%)
  other arithmetic  6.53 us (2%)
  local copies, waits for them, and re-layouts  4.6 us (1%)
    all_gather x1, waiting for transfers between devices, on_device(): lax.all_gather(gate_weight, 'sp', axis=0, tiled=True)  94.5 us
    all_gather x1, waiting for transfers between devices, on_device(): down_whole = lax.all_gather(down_weight, 'sp', axis=1, tiled=True)  93.2 us
    all_gather x1, waiting for transfers between devices, on_device(): lax.all_gather(up_weight, 'sp', axis=0, tiled=True)  87.8 us
    all_gather x1, waiting for transfers between devices, end_stops_all(): out_arr = lax.all_gather(new, axis_name='sp', axis=0, tiled=True)  41 us
    reduce_scatter x1, waiting for transfers between devices, on_device(): lax.psum_scatter(jnp.dot(picked, down_whole, preferred_element_type=jnp.f...  23.1 us
    all_gather x1, waiting for transfers between devices, on_device(): gathered = lax.all_gather(normed_in, 'tp', axis=0, tiled=True)  12.9 us
    dot_general x1, matrix products, on_device(): jnp.dot(picked, down_whole, preferred_element_type=jnp.float32)  8.92 us
  transfers between devices with their start and end apart: 6, of which 6 were waited for; matrix products, arithmetic and copies ran while one was open for 1% of the time, Pallas kernels for 0%

profile of v1, /device:TPU:0, one launch (start us, length us, event | category | flops | bytes accessed | tf_op | source)
XLA Modules:
  0.0 407.1 jit_solution(8910368274869061140)
XLA Ops:
  6.5 0.9 copy.14
  7.5 0.9 copy.15
  8.4 0.7 pad_maximum_fusion
  9.1 0.0 all-gather.6.cloned.1.call-update
  9.1 0.0 all-gather.8.cloned.1.call-start
  9.2 1.0 copy.16
  10.2 0.1 copy.17
  10.3 0.1 copy.18
  10.4 0.1 broadcast_bitcast_fusion
  10.5 41.0 %all-gather.6.cloned.1.call-done = bf16[2048,256]{0,1:T(8,128)(2,1)} async-done(((bf16[256,256]{0,1:T(8,128)(2,1)}), bf16[2048,256]{0,1:T(8,128)(2,1)}) %all-gather.6.cloned.1.call-update) | async-done | bytes 1048592 | tf_op jit(solution)/shard_map/all_gather | solution.py:12
  51.5 1.1 split.8
  52.6 0.7 multiply_reduce_fusion.1
  53.4 0.8 fusion
  54.1 0.7 multiply_reduce_fusion
  54.9 0.8 fusion.2
  55.7 0.9 fusion.29
  56.6 0.0 copy-start.6
  56.6 1.1 multiply_reduce_fusion.4
  57.7 0.0 copy-start.1
  57.8 0.0 copy-start.3
  57.8 0.0 copy-start.4
  57.8 0.1 multiply_convert_fusion.1
  57.9 0.1 copy.26
  58.1 0.1 reshape_reshape.3
  58.2 7.3 %all_to_all.15 = bf16[4,64,256]{2,1,0:T(8,128)(2,1)S(1)} all-to-all(bf16[4,64,256]{2,1,0:T(8,128)(2,1)S(1)} %reshape_reshape.3), channel_id=1, replica_groups=mesh['sp'=8,'tp'=4] {'tp'}, dimensions={0} | all-to-all | bytes 262144 | tf_op jit(solution)/shard_map/all_to_all | solution.py:95
  65.4 0.1 copy.20
  65.6 3.1 multiply_reduce_fusion.3
  68.8 0.3 multiply_reduce_fusion.2
  69.0 0.9 multiply_convert_fusion
  69.9 0.0 all-gather.8.cloned.1.call-update
  70.0 0.0 all-gather.10.cloned.1.call-start
  70.0 0.7 all-gather.10.cloned.1.call-update
  70.7 0.0 all-gather.12.cloned.1.call-start
  70.8 0.5 all-gather.12.cloned.1.call-update
  71.3 0.0 all-gather.14.cloned.1.call-start
  71.3 0.5 all-gather.14.cloned.1.call-update
  71.9 0.0 reduce-scatter.2.cloned.1.call-start
  71.9 12.9 %all-gather.8.cloned.1.call-done = bf16[256,2048]{1,0:T(8,128)(2,1)} async-done(((bf16[64,2048]{1,0:T(8,128)(2,1)}), bf16[256,2048]{1,0:T(8,128)(2,1)}) %all-gather.8.cloned.1.call-update) | async-done | bytes 1048592 | tf_op jit(solution)/shard_map/all_gather | solution.py:101
  84.8 94.5 %all-gather.10.cloned.1.call-done = bf16[2048,1408]{1,0:T(8,128)(2,1)} async-done(((bf16[256,1408]{1,0:T(8,128)(2,1)}), bf16[2048,1408]{1,0:T(8,128)(2,1)}) %all-gather.10.cloned.1.call-update) | async-done | bytes 5767184 | tf_op jit(solution)/shard_map/all_gather | solution.py:104
  179.3 4.8 %fusion.47 = f32[256,1408]{1,0:T(8,128)S(1)} fusion(bf16[256,2048]{1,0:T(8,128)(2,1)} %all-gather.8.cloned.1.call-done, bf16[2048,1408]{1,0:T(8,128)(2,1)} %all-gather.10.cloned.1.call-done), kind=kOutput, calls=%fused_computation.61 | convolution fusion | flops 1476395008 | bytes 8257536 | tf_op jit(solution)/shard_map/dot_general | solution.py:108
  184.1 0.0 copy-start.5
  184.1 87.8 %all-gather.12.cloned.1.call-done = bf16[2048,1408]{1,0:T(8,128)(2,1)} async-done(((bf16[256,1408]{1,0:T(8,128)(2,1)}), bf16[2048,1408]{1,0:T(8,128)(2,1)}) %all-gather.12.cloned.1.call-update) | async-done | bytes 5767184 | tf_op jit(solution)/shard_map/all_gather | solution.py:105
  271.9 93.2 %all-gather.14.cloned.1.call-done = bf16[1408,2048]{1,0:T(8,128)(2,1)} async-done(((bf16[1408,256]{1,0:T(8,128)(2,1)}), bf16[1408,2048]{1,0:T(8,128)(2,1)}) %all-gather.14.cloned.1.call-update) | async-done | bytes 5767184 | tf_op jit(solution)/shard_map/all_gather | solution.py:112
  365.1 8.9 %convolution_convert_fusion = bf16[256,2048]{1,0:T(8,128)(2,1)} fusion(bf16[1408,2048]{1,0:T(8,128)(2,1)} %all-gather.14.cloned.1.call-done, bf16[256,2048]{1,0:T(8,128)(2,1)S(1)} %copy-done.7, bf16[2048,1408]{1,0:T(8,128)(2,1)} %all-gather.12.cloned.1.call-done, f32[256,1408]{1,0:T(8,128)S(1)} %fusion.47), kind=kOutput, calls=%fused_computation.10 | convolution fusion | flops 2955476992 | bytes 15073280 | tf_op jit(solution)/shard_map/dot_general | solution.py:116
  374.1 0.0 reduce-scatter.2.cloned.1.call-update
  374.1 23.1 %reduce-scatter.2.cloned.1.call-done = bf16[64,2048]{1,0:T(8,128)(2,1)} async-done(((bf16[256,2048]{1,0:T(8,128)(2,1)}), bf16[64,2048]{1,0:T(8,128)(2,1)}) %reduce-scatter.2.cloned.1.call-update) | async-done | bytes 262160 | tf_op jit(solution)/shard_map/reduce_scatter | solution.py:115
  397.2 1.1 fusion.32
  398.3 1.9 fusion.36
  (25 shorter events, 0.1 us)
Async XLA Ops:
  6.5 3.9 copy-start
  6.5 45.0 %all-gather.6.cloned.1.call-start = ((), (), s32[]{:S(2)}) async-start(), calls=%async_computation.2 | async-start | bytes 1179648 | tf_op jit(solution)/shard_map/all_gather | solution.py:12
  9.1 75.7 %all-gather.8.cloned.1.call-start = ((), (), s32[]{:S(2)}) async-start(), calls=%async_computation.3 | async-start | bytes 1310720 | tf_op jit(solution)/shard_map/all_gather | solution.py:101
  54.1 1.5 copy-start.2
  56.6 1.2 copy-start.6
  57.7 11.0 %copy-start.1 = (bf16[64,2048]{1,0:T(8,128)(2,1)S(1)}, bf16[64,2048]{1,0:T(8,128)(2,1)}, u32[]{:S(2)}) copy-start(bf16[64,2048]{1,0:T(8,128)(2,1)} %param.13) | copy-start | bytes 786436
  57.8 11.0 %copy-start.3 = (f32[2048]{0:T(1024)S(1)}, f32[2048]{0:T(1024)}, u32[]{:S(2)}) copy-start(f32[2048]{0:T(1024)} %param.20) | copy-start | bytes 24580
  57.8 11.3 %copy-start.4 = (f32[2048]{0:T(1024)S(1)}, f32[2048]{0:T(1024)}, u32[]{:S(2)}) copy-start(f32[2048]{0:T(1024)} %param.21) | copy-start | bytes 24580
  70.0 109.4 %all-gather.10.cloned.1.call-start = ((), (), s32[]{:S(2)}) async-start(), calls=%async_computation.4 | async-start | bytes 6488064 | tf_op jit(solution)/shard_map/all_gather | solution.py:104
  70.7 201.2 %all-gather.12.cloned.1.call-start = ((), (), s32[]{:S(2)}) async-start(), calls=%async_computation.5 | async-start | bytes 6488064 | tf_op jit(solution)/shard_map/all_gather | solution.py:105
  71.3 293.9 %all-gather.14.cloned.1.call-start = ((), (), s32[]{:S(2)}) async-start(), calls=%async_computation.6 | async-start | bytes 6488064 | tf_op jit(solution)/shard_map/all_gather | solution.py:112
  71.9 325.3 %reduce-scatter.2.cloned.1.call-start = ((), (), s32[]{:S(2)}) async-start(), calls=%async_computation.7 | async-start | bytes 1310720 | tf_op jit(solution)/shard_map/reduce_scatter | solution.py:115
  84.8 280.3 %copy-start.7 = (bf16[256,2048]{1,0:T(8,128)(2,1)S(1)}, bf16[256,2048]{1,0:T(8,128)(2,1)}, u32[]{:S(2)}) copy-start(bf16[256,2048]{1,0:T(8,128)(2,1)} %all-gather.8.cloned.1.call-done) | copy-start | bytes 3145732
  184.1 214.2 %copy-start.5 = (f32[2048]{0:T(1024)S(1)}, f32[2048]{0:T(1024)}, u32[]{:S(2)}) copy-start(f32[2048]{0:T(1024)} %param.22) | copy-start | bytes 24580
Sparse Core Ops, SparseCore 0:
  9.4 42.1 all-gather.5
  70.1 14.6 all-gather.7
  87.0 92.2 all-gather.9
  181.4 90.4 all-gather.11
  273.8 91.2 all-gather.13
  374.2 22.9 reduce-scatter.1
